TPU v7x, 32 devices: a whole 2x2x4 slice. The times are simulated.
32 devices in a mesh: sp: 16 (over z, y, core), tp: 2 (over x).
Axes of the slice: x: 2, y: 2, z: 4, core: 2. Of those that a mesh axis runs over, the one named last changes fastest.
Arguments:
- queries: bfloat16 [16384, 1024], P('sp', 'tp'), may hold values from -8 to 8
- keyvals: bfloat16 [16384, 8, 128], P('sp', 'tp'), may hold values from -8 to 8
- head_sink_logit: float32 [16], P('tp'), may hold values from 2 to 7
- doc_ids: int32 [16384], P('sp'), may hold values from 0 to 7, never falling along the last dimension, each value on 1 to 4096 neighbouring positions
- stream_in: bfloat16 [16384, 2048], P(('sp', 'tp')), may hold values from -6 to 6
- out_weight: bfloat16 [1024, 2048], replicated, may hold values from -1.5 to 1.5
- first_gain: float32 [2048], replicated, may hold values from 0.1 to 1.9
- up_weight: bfloat16 [2048, 8192], P('sp', 'tp'), may hold values from -0.125 to 0.125
- down_weight: bfloat16 [8192, 2048], P('tp', 'sp'), may hold values from -0.0625 to 0.0625
- second_gain: float32 [2048], replicated, may hold values from 0.1 to 1.9
Outputs:
- layer_out: bfloat16 [16384, 2048], P(('sp', 'tp'))
Inputs may be any that keep to these rules, and one draw needn't show every extreme that they name: `doc_ids`: document numbers never fall along the sequence.
All inputs are finite; a program needn't handle non-finite values.
Results may differ from a plain program's by a relative error of at most 0.013.
Values may be sent and summed in bfloat16 or wider, within the bound.
A program may use at most 128 MiB of HBM per device.

v0:
```python
import jax
import jax.numpy as jnp
from jax import lax
from jax.sharding import PartitionSpec as P

HEAD_SIZE = 64
WINDOW_REACH = 128
NEG_LARGE = -1e30
NORM_EPS = 1e-05


def padded(block, sides, width):
    for axis, dim in sides:
        count = lax.axis_size(axis)
        forward = [(i, i + 1) for i in range(count - 1)]
        backward = [(target, source) for source, target in forward]
        low = lax.ppermute(
            lax.slice_in_dim(block, block.shape[dim] - width, None, axis=dim), axis, forward
        )
        high = lax.ppermute(lax.slice_in_dim(block, 0, width, axis=dim), axis, backward)
        block = jnp.concatenate([low, block, high], axis=dim)
    return block


def layer_norm(stream, gain_row):
    centre = jnp.mean(stream, axis=-1, keepdims=True)
    shifted = stream - centre
    spread = jnp.mean(shifted * shifted, axis=-1, keepdims=True)
    return shifted * lax.rsqrt(spread + NORM_EPS) * gain_row


def attend(queries, keyvals, head_sink_logit, doc_ids):
    tok_rows = queries.shape[0]
    kv_heads = keyvals.shape[1]
    heads_per_group = queries.shape[1] // (HEAD_SIZE * kv_heads)
    block_list = tok_rows // WINDOW_REACH
    score_scale = HEAD_SIZE ** (-0.5)
    doc_marks = doc_ids.astype(jnp.bfloat16)
    rim_keys, rim_docs = (
        padded(keyvals, (("sp", 0),), WINDOW_REACH),
        padded(doc_marks, (("sp", 0),), WINDOW_REACH),
    )
    padded_rows = rim_keys.reshape(block_list + 2, WINDOW_REACH, kv_heads, 2 * HEAD_SIZE)
    banded = jnp.concatenate([padded_rows[:-2], padded_rows[1:-1], padded_rows[2:]], axis=1)
    doc_ext = rim_docs.reshape(block_list + 2, WINDOW_REACH)
    doc_band = jnp.concatenate([doc_ext[:-2], doc_ext[1:-1], doc_ext[2:]], axis=1)
    offset = lax.axis_index("sp") * tok_rows
    total_rows = tok_rows * lax.axis_size("sp")
    query_pos = offset + jnp.arange(tok_rows, dtype=jnp.int32).reshape(block_list, WINDOW_REACH, 1)
    key_pos = (
        offset
        + (
            jnp.arange(block_list, dtype=jnp.int32)[:, None] * WINDOW_REACH
            + jnp.arange(3 * WINDOW_REACH, dtype=jnp.int32)[None, :]
            - WINDOW_REACH
        )[:, None, :]
    )
    allowed = (
        (jnp.abs(query_pos - key_pos) <= WINDOW_REACH)
        & (key_pos >= 0)
        & (key_pos < total_rows)
        & (doc_marks.reshape(block_list, WINDOW_REACH, 1) == doc_band[:, None, :])
    )
    query_block_list = queries.reshape(
        block_list, WINDOW_REACH, kv_heads, heads_per_group, HEAD_SIZE
    )
    scores = (
        jnp.einsum(
            "nqhgd,nkhd->nhgqk",
            query_block_list,
            banded[..., :HEAD_SIZE],
            preferred_element_type=jnp.float32,
        )
        * score_scale
    )
    scores = jnp.where(allowed[:, None, None], scores, NEG_LARGE)
    sink_col = head_sink_logit.reshape(kv_heads, heads_per_group)[None, :, :, None, None]
    highest = jnp.maximum(jnp.max(scores, axis=-1, keepdims=True), sink_col)
    powers = jnp.exp(scores - highest)
    denominator = jnp.sum(powers, axis=-1, keepdims=True) + jnp.exp(sink_col - highest)
    weights = (powers / denominator).astype(jnp.bfloat16)
    mixed_out = jnp.einsum(
        "nhgqk,nkhd->nqhgd", weights, banded[..., HEAD_SIZE:], preferred_element_type=jnp.float32
    )
    return mixed_out.astype(jnp.bfloat16).reshape(tok_rows, kv_heads * heads_per_group * HEAD_SIZE)


def per_device(
    queries,
    keyvals,
    head_sink_logit,
    doc_ids,
    stream_in,
    out_weight,
    first_gain,
    up_weight,
    down_weight,
    second_gain,
):
    up_whole = lax.all_gather(up_weight, "sp", axis=0, tiled=True)
    down_whole = lax.all_gather(down_weight, "sp", axis=1, tiled=True)
    attended = attend(queries, keyvals, head_sink_logit, doc_ids)
    tp_count = lax.axis_size("tp")
    own_rows = attended.shape[0] // tp_count
    by_peer = attended.reshape(tp_count, own_rows, attended.shape[1])
    projected = jnp.dot(
        lax.all_to_all(by_peer, "tp", split_axis=0, concat_axis=2, tiled=True)[0],
        out_weight,
        preferred_element_type=jnp.float32,
    )[None][0]
    first_stream = layer_norm(stream_in.astype(jnp.float32) + projected, first_gain).astype(
        jnp.bfloat16
    )
    hidden = jnp.dot(
        lax.all_gather(first_stream, "tp", axis=0, tiled=True),
        up_whole,
        preferred_element_type=jnp.float32,
    )
    active = jnp.square(jnp.maximum(hidden, 0.0)).astype(jnp.bfloat16)
    mixed_out = lax.psum_scatter(
        jnp.dot(active, down_whole, preferred_element_type=jnp.float32).astype(jnp.bfloat16),
        "tp",
        scatter_dimension=0,
        tiled=True,
    ).astype(jnp.float32)
    return layer_norm(first_stream.astype(jnp.float32) + mixed_out, second_gain).astype(
        jnp.bfloat16
    )


def solution(mesh):
    return jax.shard_map(
        per_device,
        mesh=mesh,
        in_specs=(
            P("sp", "tp"),
            P("sp", "tp", None),
            P("tp"),
            P("sp"),
            P(("sp", "tp"), None),
            P(),
            P(),
            P("sp", "tp"),
            P("tp", "sp"),
            P(),
        ),
        out_specs=P(("sp", "tp"), None),
        check_vma=False,
    )
```

profile of v0, /device:TPU:0, one launch (start us, length us, event | category | flops | bytes accessed | tf_op | source)
XLA Modules:
  0.0 477.8 jit_solution(12057201046544516895)
XLA Ops:
  6.5 0.0 all-gather.4.cloned.1.call-start
  6.5 0.8 convert_element_type.34
  7.3 2.4 collective-permute-start.2
  9.7 1.3 collective-permute-start.3
  11.0 1.4 copy.26
  12.4 5.8 %collective-permute-start = (bf16[128,4,128]{2,0,1:T(8,128)(2,1)S(1)}, bf16[128,4,128]{2,0,1:T(8,128)(2,1)}, u32[]{:S(2)}, u32[]{:S(2)}) collective-permute-start(bf16[128,4,128]{2,0,1:T(8,128)(2,1)S(1)} %get-tuple-element.7), channel_id=1, source_target_pairs={{0,2},{2,4},{4,6},{6,8},{8,10},{10,12},{12,14},{14,16},{16,18},{18... | collective-permute-start | bytes 393224 | tf_op jit(solution)/shard_map/ppermute | solution.py:17
  18.2 1.3 collective-permute-start.1
  19.5 0.7 convert_bitcast_fusion
  20.2 0.1 fusion.13
  20.3 0.1 add_add_fusion
  20.4 2.3 copy.32
  22.6 0.0 copy-done.7
  22.6 2.1 reshape.167
  24.7 0.0 copy-done.10
  24.7 0.1 max.24
  24.8 0.0 collective-permute-done.2
  24.8 0.0 collective-permute-done.3
  24.8 2.3 fusion.9
  27.1 0.0 collective-permute-done
  27.1 0.0 collective-permute-done.1
  27.1 1.3 pad_maximum_fusion.2
  28.4 0.7 copy.31
  29.1 0.7 copy.33
  29.7 0.0 copy-start.6
  29.7 1.8 pad_maximum_fusion
  31.6 0.1 copy-done.6
  31.6 2.5 fusion.1
  34.2 0.0 copy-done.4
  34.2 0.1 broadcast_maximum_fusion
  34.3 0.0 copy-start.5
  34.3 3.4 fusion
  37.7 0.1 exponential_add_fusion
  37.8 0.0 copy-done.5
  37.8 3.6 fusion.11
  41.4 0.7 copy.37
  42.1 0.4 reshape_reshape.3
  42.6 0.0 copy-start.3
  42.6 0.2 copy.38
  42.8 17.2 %all_to_all.15 = bf16[2,512,512]{1,2,0:T(8,128)(2,1)S(1)} all-to-all(bf16[2,512,512]{1,2,0:T(8,128)(2,1)S(1)} %copy.38), channel_id=1, replica_groups=mesh['sp'=16,'tp'=2] {'tp'}, dimensions={0} | all-to-all | bytes 2097152 | tf_op jit(solution)/shard_map/all_to_all | solution.py:107
  60.0 4.2 fusion.20
  64.2 0.0 copy-start.8
  64.2 0.6 multiply_reduce_fusion.1
  64.8 1.4 copy-done
  66.1 1.9 multiply_convert_fusion.2
  68.1 0.0 all-gather.4.cloned.1.call-update
  68.1 0.0 all-gather.6.cloned.1.call-start
  68.1 0.7 all-gather.6.cloned.1.call-update
  68.8 0.0 all-gather.8.cloned.1.call-start
  68.9 0.7 all-gather.8.cloned.1.call-update
  69.6 0.0 reduce-scatter.2.cloned.1.call-start
  69.6 56.9 %all-gather.4.cloned.1.call-done = bf16[1024,2048]{1,0:T(8,128)(2,1)} async-done(((bf16[512,2048]{1,0:T(8,128)(2,1)}), bf16[1024,2048]{1,0:T(8,128)(2,1)}) %all-gather.4.cloned.1.call-update) | async-done | bytes 4194320 | tf_op jit(solution)/shard_map/all_gather | solution.py:115
  126.5 128.6 %all-gather.6.cloned.1.call-done = bf16[2048,4096]{1,0:T(8,128)(2,1)} async-done(((bf16[128,4096]{1,0:T(8,128)(2,1)}), bf16[2048,4096]{1,0:T(8,128)(2,1)}) %all-gather.6.cloned.1.call-update) | async-done | bytes 16777232 | tf_op jit(solution)/shard_map/all_gather | solution.py:100
  255.1 22.9 %fusion.44 = bf16[1024,4096]{1,0:T(8,128)(2,1)} fusion(bf16[2048,4096]{1,0:T(8,128)(2,1)} %all-gather.6.cloned.1.call-done, bf16[1024,2048]{1,0:T(8,128)(2,1)} %all-gather.4.cloned.1.call-done), kind=kOutput, calls=%bitcast_fusion.1.clone.1 | convolution fusion | flops 17192452096 | bytes 29360128 | tf_op jit(solution)/shard_map/dot_general | solution.py:114
  278.0 107.4 %all-gather.8.cloned.1.call-done = bf16[4096,2048]{1,0:T(8,128)(2,1)} async-done(((bf16[4096,128]{1,0:T(8,128)(2,1)}), bf16[4096,2048]{1,0:T(8,128)(2,1)}) %all-gather.8.cloned.1.call-update) | async-done | bytes 16777232 | tf_op jit(solution)/shard_map/all_gather | solution.py:101
  385.4 23.7 %convolution_convert_fusion = bf16[1024,2048]{1,0:T(8,128)(2,1)} fusion(bf16[4096,2048]{1,0:T(8,128)(2,1)} %all-gather.8.cloned.1.call-done, bf16[1024,4096]{1,0:T(8,128)(2,1)} %fusion.44), kind=kOutput, calls=%fused_computation.15 | convolution fusion | flops 17181966336 | bytes 29360128 | tf_op jit(solution)/shard_map/dot_general | solution.py:121
  409.1 0.0 reduce-scatter.2.cloned.1.call-update
  409.1 52.7 %reduce-scatter.2.cloned.1.call-done = bf16[512,2048]{1,0:T(8,128)(2,1)} async-done(((bf16[1024,2048]{1,0:T(8,128)(2,1)}), bf16[512,2048]{1,0:T(8,128)(2,1)}) %reduce-scatter.2.cloned.1.call-update) | async-done | bytes 2097168 | tf_op jit(solution)/shard_map/reduce_scatter | solution.py:120
  461.8 3.9 fusion.4
  465.7 0.0 copy-start.9
  465.8 0.1 copy-done.1
  465.8 0.7 copy-done.2
  466.5 1.2 multiply_reduce_fusion
  467.8 0.0 copy-done.9
  467.8 3.5 multiply_convert_fusion.1
  (18 shorter events, 0.1 us)
Async XLA Ops:
  6.5 16.1 %copy-start.7 = (bf16[1024,512]{1,0:T(8,128)(2,1)S(1)}, bf16[1024,512]{1,0:T(8,128)(2,1)}, u32[]{:S(2)}) copy-start(bf16[1024,512]{1,0:T(8,128)(2,1)} %param.10) | copy-start | bytes 3145732
  6.5 18.2 %copy-start.10 = (f32[8]{0:T(128)S(1)}, f32[8]{0:T(128)}, u32[]{:S(2)}) copy-start(f32[8]{0:T(128)} %param.12) | copy-start | bytes 100
  6.5 119.9 %all-gather.4.cloned.1.call-start = ((), (), s32[]{:S(2)}) async-start(), calls=%async_computation.2 | async-start | bytes 6291456 | tf_op jit(solution)/shard_map/all_gather | solution.py:115
  7.3 17.5 %collective-permute-start.2 = (bf16[128]{0:T(256)(128)(2,1)S(1)}, bf16[128]{0:T(256)(128)(2,1)S(1)}, u32[]{:S(2)}, u32[]{:S(2)}) collective-permute-start(bf16[128]{0:T(256)(128)(2,1)S(1)} %get-tuple-element.11), channel_id=1, source_target_pairs={{0,2},{2,4},{4,6},{6,8},{8,10},{10,12},{12,14},{14,16},{16,18},{18... | collective-permute-start | bytes 776 | tf_op jit(solution)/shard_map/ppermute | solution.py:17
  9.7 15.1 %collective-permute-start.3 = (bf16[128]{0:T(256)(128)(2,1)S(1)}, bf16[128]{0:T(256)(128)(2,1)S(1)}, u32[]{:S(2)}, u32[]{:S(2)}) collective-permute-start(bf16[128]{0:T(256)(128)(2,1)S(1)} %get-tuple-element.12), channel_id=1, source_target_pairs={{2,0},{4,2},{6,4},{8,6},{10,8},{12,10},{14,12},{16,14},{18,16},{20... | collective-permute-start | bytes 776 | tf_op jit(solution)/shard_map/ppermute | solution.py:20
  12.4 14.7 %collective-permute-start = (bf16[128,4,128]{2,0,1:T(8,128)(2,1)S(1)}, bf16[128,4,128]{2,0,1:T(8,128)(2,1)}, u32[]{:S(2)}, u32[]{:S(2)}) collective-permute-start(bf16[128,4,128]{2,0,1:T(8,128)(2,1)S(1)} %get-tuple-element.7), channel_id=1, source_target_pairs={{0,2},{2,4},{4,6},{6,8},{8,10},{10,12},{12,14},{14,16},{16,18},{18... | collective-permute-start | bytes 393224 | tf_op jit(solution)/shard_map/ppermute | solution.py:17
  18.2 8.9 %collective-permute-start.1 = (bf16[128,4,128]{2,0,1:T(8,128)(2,1)S(1)}, bf16[128,4,128]{2,0,1:T(8,128)(2,1)}, u32[]{:S(2)}, u32[]{:S(2)}) collective-permute-start(bf16[128,4,128]{2,0,1:T(8,128)(2,1)S(1)} %get-tuple-element.8), channel_id=1, source_target_pairs={{2,0},{4,2},{6,4},{8,6},{10,8},{12,10},{14,12},{16,14},{18,16},{20... | collective-permute-start | bytes 393224 | tf_op jit(solution)/shard_map/ppermute | solution.py:20
  29.7 1.9 copy-start.6
  31.6 2.5 copy-start.4
  34.3 3.6 copy-start.5
  42.6 17.4 %copy-start.3 = (bf16[1024,2048]{1,0:T(8,128)(2,1)S(1)}, bf16[1024,2048]{1,0:T(8,128)(2,1)}, u32[]{:S(2)}) copy-start(bf16[1024,2048]{1,0:T(8,128)(2,1)} %param.15) | copy-start | bytes 12582916
  64.2 1.9 copy-start
  64.2 1.9 copy-start.8
  68.1 187.0 %all-gather.6.cloned.1.call-start = ((), (), s32[]{:S(2)}) async-start(), calls=%async_computation.3 | async-start | bytes 17825792 | tf_op jit(solution)/shard_map/all_gather | solution.py:100
  68.8 316.5 %all-gather.8.cloned.1.call-start = ((), (), s32[]{:S(2)}) async-start(), calls=%async_computation.4 | async-start | bytes 17825792 | tf_op jit(solution)/shard_map/all_gather | solution.py:101
  69.6 392.2 %reduce-scatter.2.cloned.1.call-start = ((), (), s32[]{:S(2)}) async-start(), calls=%async_computation.5 | async-start | bytes 6291456 | tf_op jit(solution)/shard_map/reduce_scatter | solution.py:120
  461.8 4.0 copy-start.1
  461.8 4.7 copy-start.2
  465.7 2.0 copy-start.9
Sparse Core Ops, SparseCore 0:
  68.2 58.2 all-gather.3
  128.6 126.4 all-gather.5
  257.3 128.0 all-gather.7
  409.2 52.5 reduce-scatter.1
where the time goes:
time: 478 us
  waiting for transfers between devices  347 us (73%)
  matrix products  56.9 us (12%)
  other arithmetic  21.8 us (5%)
  blocking collectives  17.2 us (4%)
  between operations  13.4 us (3%)
  starting transfers between devices  10.9 us (2%)
  local copies, waits for them, and re-layouts  10.6 us (2%)
    all_gather x1, waiting for transfers between devices, per_device(): up_whole = lax.all_gather(up_weight, 'sp', axis=0, tiled=True)  129 us
    all_gather x1, waiting for transfers between devices, per_device(): down_whole = lax.all_gather(down_weight, 'sp', axis=1, tiled=True)  107 us
    all_gather x1, waiting for transfers between devices, per_device(): lax.all_gather(first_stream, 'tp', axis=0, tiled=True)  56.9 us
    reduce_scatter x1, waiting for transfers between devices, per_device(): lax.psum_scatter(jnp.dot(active, down_whole, preferred_element_type=jnp.f...  52.7 us
    dot_general x1, matrix products, per_device(): jnp.dot(active, down_whole, preferred_element_type=jnp.float32)  23.7 us
    dot_general x1, matrix products, per_device(): jnp.dot(lax.all_gather(first_stream, 'tp', axis=0, tiled=True), up_whole,...  22.9 us
    all_to_all x1, blocking collectives, per_device(): lax.all_to_all(by_peer, 'tp', split_axis=0, concat_axis=2, tiled=True)[0]  17.2 us
  transfers between devices with their start and end apart: 8, of which 4 were waited for; matrix products, arithmetic and copies ran while one was open for 7% of the time, Pallas kernels for 0%

commit v1 on v0

--- a/solution.py
+++ b/solution.py
@@ -97,7 +97,10 @@
     down_weight,
     second_gain,
 ):
-    up_whole = lax.all_gather(up_weight, "sp", axis=0, tiled=True)
+    size = lax.axis_size("sp")
+    parts = jnp.stack([up_weight for _ in range(size)])
+    parts = lax.all_to_all(parts, "sp", split_axis=0, concat_axis=0)
+    up_whole = jnp.concatenate(parts, axis=0)
     down_whole = lax.all_gather(down_weight, "sp", axis=1, tiled=True)
     attended = attend(queries, keyvals, head_sink_logit, doc_ids)
     tp_count = lax.axis_size("tp")

time: 478 us -> 662 us (1.38)
  waiting for transfers between devices: 347 us -> 517 us
  starting transfers between devices: 10.9 us -> 18.8 us
  local copies, waits for them, and re-layouts: 10.6 us -> 17.4 us
    all_to_all x0 -> x1, waiting for transfers between devices: none -> 351 us  [per_device(): parts = lax.all_to_all(parts, 'sp', split_axis=0, concat_axis=0)]
    all_gather x1 -> x0, waiting for transfers between devices: 129 us -> none  [per_device(): up_whole = lax.all_gather(up_weight, 'sp', axis=0, tiled=True)]
    all_gather x1, waiting for transfers between devices: 107 us -> 0.01 us  [per_device(): down_whole = lax.all_gather(down_weight, 'sp', axis=1, tiled=True)]
    reduce_scatter x1, waiting for transfers between devices: 52.7 us -> 121 us  [per_device(): lax.psum_scatter(jnp.dot(active, down_whole, preferred_element_type=jnp.f...]
    all_gather x1, waiting for transfers between devices: 56.9 us -> 44.3 us  [per_device(): lax.all_gather(first_stream, 'tp', axis=0, tiled=True)]
    all_to_all x0 -> x1, starting transfers between devices: none -> 8.59 us  [per_device(): parts = lax.all_to_all(parts, 'sp', split_axis=0, concat_axis=0)]
  transfers between devices with their start and end apart: 8 -> 8, of which waited for: 4 -> 3; matrix products, arithmetic and copies ran while one was open for 7% -> 6% of each run, Pallas kernels for 0% -> 0%
where the time goes in v1:
time: 662 us
  waiting for transfers between devices  517 us (78%)
  matrix products  56.9 us (9%)
  other arithmetic  21.8 us (3%)
  starting transfers between devices  18.8 us (3%)
  local copies, waits for them, and re-layouts  17.4 us (3%)
  blocking collectives  16.5 us (2%)
  between operations  13.4 us (2%)
    all_to_all x1, waiting for transfers between devices, per_device(): parts = lax.all_to_all(parts, 'sp', split_axis=0, concat_axis=0)  351 us
    reduce_scatter x1, waiting for transfers between devices, per_device(): lax.psum_scatter(jnp.dot(active, down_whole, preferred_element_type=jnp.f...  121 us
    all_gather x1, waiting for transfers between devices, per_device(): lax.all_gather(first_stream, 'tp', axis=0, tiled=True)  44.3 us
    dot_general x1, matrix products, per_device(): jnp.dot(active, down_whole, preferred_element_type=jnp.float32)  23.7 us
    dot_general x1, matrix products, per_device(): jnp.dot(lax.all_gather(first_stream, 'tp', axis=0, tiled=True), up_whole,...  22.9 us
    all_to_all x1, blocking collectives, per_device(): lax.all_to_all(by_peer, 'tp', split_axis=0, concat_axis=2, tiled=True)[0]  16.5 us
  transfers between devices with their start and end apart: 8, of which 3 were waited for; matrix products, arithmetic and copies ran while one was open for 6% of the time, Pallas kernels for 0%

profile of v1, /device:TPU:0, one launch (start us, length us, event | category | flops | bytes accessed | tf_op | source)
XLA Modules:
  0.0 661.7 jit_solution(14333733363191048357)
XLA Ops:
  6.5 0.0 all-gather.3.cloned.1.call-start
  6.5 0.8 convert_element_type.34
  7.3 2.4 collective-permute-start.2
  9.7 1.3 collective-permute-start.3
  11.0 1.4 copy.26
  12.4 5.2 collective-permute-start
  17.6 1.3 collective-permute-start.1
  18.9 0.7 convert_bitcast_fusion
  19.6 0.1 fusion.13
  19.7 0.1 add_add_fusion
  19.7 2.3 copy.32
  22.0 0.0 copy-done.7
  22.0 2.1 reshape.173
  24.1 0.1 max.24
  24.2 0.0 collective-permute-done.2
  24.2 0.0 collective-permute-done.3
  24.2 2.3 fusion.9
  26.5 0.0 collective-permute-done
  26.5 0.0 copy-start.10
  26.5 0.7 copy-done.10
  27.2 0.0 collective-permute-done.1
  27.2 1.2 pad_maximum_fusion.2
  28.4 0.7 copy.31
  29.1 0.7 copy.33
  29.8 0.0 copy-start.6
  29.8 1.8 pad_maximum_fusion
  31.6 0.1 copy-done.6
  31.7 2.5 fusion.1
  34.2 0.1 broadcast_maximum_fusion
  34.3 0.0 copy-start.5
  34.3 3.4 fusion
  37.8 0.1 exponential_add_fusion
  37.9 0.0 copy-done.5
  37.9 3.6 fusion.11
  41.5 0.7 copy.37
  42.2 0.4 reshape_reshape.3
  42.6 0.0 copy-start.3
  42.6 0.2 copy.38
  42.8 16.5 %all_to_all.20 = bf16[2,512,512]{1,2,0:T(8,128)(2,1)S(1)} all-to-all(bf16[2,512,512]{1,2,0:T(8,128)(2,1)S(1)} %copy.38), channel_id=1, replica_groups=mesh['sp'=16,'tp'=2] {'tp'}, dimensions={0} | all-to-all | bytes 2097152 | tf_op jit(solution)/shard_map/all_to_all | solution.py:110
  59.4 0.0 copy-done.3
  59.4 4.2 fusion.20
  63.6 0.0 copy-start.9
  63.6 0.6 multiply_reduce_fusion.1
  64.2 1.5 copy-done
  65.7 1.9 multiply_convert_fusion.2
  67.6 0.0 all-gather.3.cloned.1.call-update
  67.6 0.0 copy-done.8
  67.6 5.9 stack.2
  73.6 8.6 %all-to-all-start.1 = ((bf16[16,128,4096]{2,1,0:T(8,128)(2,1)}), bf16[16,128,4096]{2,1,0:T(8,128)(2,1)}, u32[]{:S(2)}, u32[]{:S(2)}) async-start(bf16[16,128,4096]{2,1,0:T(8,128)(2,1)} %stack.2), calls=%async_computation.1 | async-start | bytes 33554432 | tf_op jit(solution)/shard_map/all_to_all | solution.py:102
  82.2 0.0 all-gather.5.cloned.1.call-start
  82.2 0.7 all-gather.5.cloned.1.call-update
  82.9 0.0 reduce-scatter.2.cloned.1.call-start
  83.0 44.3 %all-gather.3.cloned.1.call-done = bf16[1024,2048]{1,0:T(8,128)(2,1)} async-done(((bf16[512,2048]{1,0:T(8,128)(2,1)}), bf16[1024,2048]{1,0:T(8,128)(2,1)}) %all-gather.3.cloned.1.call-update) | async-done | bytes 4194320 | tf_op jit(solution)/shard_map/all_gather | solution.py:118
  127.3 350.9 %all-to-all-done.1 = bf16[16,128,4096]{2,1,0:T(8,128)(2,1)} async-done(((bf16[16,128,4096]{2,1,0:T(8,128)(2,1)}), bf16[16,128,4096]{2,1,0:T(8,128)(2,1)}, u32[]{:S(2)}, u32[]{:S(2)}) %all-to-all-start.1) | async-done | bytes 16777248 | tf_op jit(solution)/shard_map/all_to_all | solution.py:102
  478.2 22.9 %fusion.44 = bf16[1024,4096]{1,0:T(8,128)(2,1)} fusion(bf16[2048,4096]{1,0:T(8,128)(2,1)} %bitcast.15, bf16[1024,2048]{1,0:T(8,128)(2,1)} %all-gather.3.cloned.1.call-done), kind=kOutput, calls=%bitcast_fusion.1.clone.1 | convolution fusion | flops 17192452096 | bytes 29360128 | tf_op jit(solution)/shard_map/dot_general | solution.py:117
  501.1 23.7 %convolution_convert_fusion = bf16[1024,2048]{1,0:T(8,128)(2,1)} fusion(bf16[4096,2048]{1,0:T(8,128)(2,1)} %all-gather.5.cloned.1.call-done, bf16[1024,4096]{1,0:T(8,128)(2,1)} %fusion.44), kind=kOutput, calls=%fused_computation.15 | convolution fusion | flops 17181966336 | bytes 29360128 | tf_op jit(solution)/shard_map/dot_general | solution.py:124
  524.7 0.0 reduce-scatter.2.cloned.1.call-update
  524.8 120.9 %reduce-scatter.2.cloned.1.call-done = bf16[512,2048]{1,0:T(8,128)(2,1)} async-done(((bf16[1024,2048]{1,0:T(8,128)(2,1)}), bf16[512,2048]{1,0:T(8,128)(2,1)}) %reduce-scatter.2.cloned.1.call-update) | async-done | bytes 2097168 | tf_op jit(solution)/shard_map/reduce_scatter | solution.py:123
  645.6 3.9 fusion.4
  649.6 0.0 copy-start.11
  649.6 0.1 copy-done.1
  649.7 0.7 copy-done.2
  650.3 1.2 multiply_reduce_fusion
  651.6 3.5 multiply_convert_fusion.1
  (22 shorter events, 0.1 us)
Async XLA Ops:
  6.5 15.5 %copy-start.7 = (bf16[1024,512]{1,0:T(8,128)(2,1)S(1)}, bf16[1024,512]{1,0:T(8,128)(2,1)}, u32[]{:S(2)}) copy-start(bf16[1024,512]{1,0:T(8,128)(2,1)} %param.10) | copy-start | bytes 3145732
  6.5 17.6 %copy-start.12 = (f32[8]{0:T(128)S(1)}, f32[8]{0:T(128)}, u32[]{:S(2)}) copy-start(f32[8]{0:T(128)} %param.12) | copy-start | bytes 100
  6.5 120.7 %all-gather.3.cloned.1.call-start = ((), (), s32[]{:S(2)}) async-start(), calls=%async_computation.3 | async-start | bytes 6291456 | tf_op jit(solution)/shard_map/all_gather | solution.py:118
  7.3 16.8 %collective-permute-start.2 = (bf16[128]{0:T(256)(128)(2,1)S(1)}, bf16[128]{0:T(256)(128)(2,1)S(1)}, u32[]{:S(2)}, u32[]{:S(2)}) collective-permute-start(bf16[128]{0:T(256)(128)(2,1)S(1)} %get-tuple-element.11), channel_id=1, source_target_pairs={{0,2},{2,4},{4,6},{6,8},{8,10},{10,12},{12,14},{14,16},{16,18},{18... | collective-permute-start | bytes 776 | tf_op jit(solution)/shard_map/ppermute | solution.py:17
  9.7 14.5 %collective-permute-start.3 = (bf16[128]{0:T(256)(128)(2,1)S(1)}, bf16[128]{0:T(256)(128)(2,1)S(1)}, u32[]{:S(2)}, u32[]{:S(2)}) collective-permute-start(bf16[128]{0:T(256)(128)(2,1)S(1)} %get-tuple-element.12), channel_id=1, source_target_pairs={{2,0},{4,2},{6,4},{8,6},{10,8},{12,10},{14,12},{16,14},{18,16},{20... | collective-permute-start | bytes 776 | tf_op jit(solution)/shard_map/ppermute | solution.py:20
  12.4 14.1 %collective-permute-start = (bf16[128,4,128]{2,0,1:T(8,128)(2,1)S(1)}, bf16[128,4,128]{2,0,1:T(8,128)(2,1)S(1)}, u32[]{:S(2)}, u32[]{:S(2)}) collective-permute-start(bf16[128,4,128]{2,0,1:T(8,128)(2,1)S(1)} %get-tuple-element.7), channel_id=1, source_target_pairs={{0,2},{2,4},{4,6},{6,8},{8,10},{10,12},{12,14},{14,16},{16,18},{18... | collective-permute-start | bytes 393224 | tf_op jit(solution)/shard_map/ppermute | solution.py:17
  17.6 9.6 %collective-permute-start.1 = (bf16[128,4,128]{2,0,1:T(8,128)(2,1)S(1)}, bf16[128,4,128]{2,0,1:T(8,128)(2,1)}, u32[]{:S(2)}, u32[]{:S(2)}) collective-permute-start(bf16[128,4,128]{2,0,1:T(8,128)(2,1)S(1)} %get-tuple-element.8), channel_id=1, source_target_pairs={{2,0},{4,2},{6,4},{8,6},{10,8},{12,10},{14,12},{16,14},{18,16},{20... | collective-permute-start | bytes 393224 | tf_op jit(solution)/shard_map/ppermute | solution.py:20
  26.5 0.7 copy-start.10
  29.8 1.9 copy-start.6
  31.7 2.6 copy-start.4
  34.3 3.6 copy-start.5
  42.6 16.7 %copy-start.3 = (bf16[1024,2048]{1,0:T(8,128)(2,1)S(1)}, bf16[1024,2048]{1,0:T(8,128)(2,1)}, u32[]{:S(2)}) copy-start(bf16[1024,2048]{1,0:T(8,128)(2,1)} %param.15) | copy-start | bytes 12582916
  63.6 2.1 copy-start
  63.6 2.1 copy-start.9
  65.6 2.0 copy-start.8
  73.6 404.6 %all-to-all-start.1 = ((bf16[16,128,4096]{2,1,0:T(8,128)(2,1)}), bf16[16,128,4096]{2,1,0:T(8,128)(2,1)}, u32[]{:S(2)}, u32[]{:S(2)}) async-start(bf16[16,128,4096]{2,1,0:T(8,128)(2,1)} %stack.2), calls=%async_computation.1 | async-start | bytes 33554432 | tf_op jit(solution)/shard_map/all_to_all | solution.py:102
  82.2 418.9 %all-gather.5.cloned.1.call-start = ((), (), s32[]{:S(2)}) async-start(), calls=%async_computation.4 | async-start | bytes 17825792 | tf_op jit(solution)/shard_map/all_gather | solution.py:104
  82.9 562.7 %reduce-scatter.2.cloned.1.call-start = ((), (), s32[]{:S(2)}) async-start(), calls=%async_computation.5 | async-start | bytes 6291456 | tf_op jit(solution)/shard_map/reduce_scatter | solution.py:123
  645.6 4.0 copy-start.1
  645.6 4.7 copy-start.2
  649.6 2.0 copy-start.11
Sparse Core Ops, SparseCore 0:
  67.7 59.4 all-gather.2
  129.4 357.9 all-gather.4
  524.9 120.6 reduce-scatter.1
